TPU v7x, 32 devices: a whole 2x2x4 slice. The times are simulated.
32 devices in a mesh: grp: 2 (over y), ep: 4 (over z), tp: 4 (over x, core).
Axes of the slice: x: 2, y: 2, z: 4, core: 2. Of those that a mesh axis runs over, the one named last changes fastest.
Arguments:
- mixer_input: bfloat16 [4096, 2048], P(('grp', 'ep', 'tp')), parts along dimension 0, may hold values from -8 to 8
- forget_cumsum: float32 [8, 4096], P('tp', 'grp'), parts along dimension 1, may hold values from -259 to 0, as said below
- mixer_gain: float32 [2048], replicated, may hold values from 0.1 to 1.9
- query_weight: bfloat16 [2048, 1024], P(None, 'tp'), may hold values from -6 to 6
- key_weight: bfloat16 [2048, 1024], P(None, 'tp'), may hold values from -6 to 6
- value_weight: bfloat16 [2048, 1024], P(None, 'tp'), may hold values from -0.125 to 0.125
- out_weight: bfloat16 [1024, 2048], P('tp'), may hold values from -0.1875 to 0.1875
- post_gain: float32 [2048], replicated, may hold values from 0.1 to 1.9
- expert_input: bfloat16 [4096, 2048], P(('grp', 'ep', 'tp')), parts along dimension 0, may hold values from -6 to 6
- expert_gain: float32 [2048], replicated, may hold values from 0.1 to 1.9
- routes: int32 [4096, 2], P(('grp', 'ep', 'tp')), parts along dimension 0, may hold values from 0 to 3, all different within a row; in each aligned block of 128 rows (0 to 127, 128 to 255, ...) at most 72 rows name the same one
- route_weight: float32 [4096, 2], P(('grp', 'ep', 'tp')), parts along dimension 0, may hold values from 0.2 to 1
- expert_gate: bfloat16 [4, 2048, 2048], P('ep', None, 'tp'), may hold values from -0.125 to 0.125
- expert_upward: bfloat16 [4, 2048, 2048], P('ep', None, 'tp'), may hold values from -0.125 to 0.125
- expert_down: bfloat16 [4, 2048, 2048], P('ep', 'tp'), may hold values from -0.125 to 0.125
Outputs:
- mixer_output: bfloat16 [4096, 2048], P(('grp', 'ep', 'tp')), parts along dimension 0
- expert_output: bfloat16 [4096, 2048], P(('grp', 'ep', 'tp')), parts along dimension 0
There are 2 independent parts, one for each index of `grp`. A program takes and returns all parts, laid end to end along the dimension named above; an argument that names none is the same for every part. Nothing has to cross between parts.
Inputs may be any that keep to these rules, and one draw needn't show every extreme that they name: `forget_cumsum`: each head's row never rises along positions. `routes`: A row names 2 different experts. Within the rows of one device (aligned blocks of 128 rows) no expert is named by more than 72 rows, and in every draw some expert is named by exactly 72 rows of some block.
All inputs are finite; a program needn't handle non-finite values.
Results may differ from a plain program's by a relative error of at most 0.012.
Values may be sent and summed in bfloat16 or wider, within the bound.
A program may use at most 128 MiB of HBM per device.

v0:
```python
import jax
import jax.numpy as jnp
from jax import lax
from jax.sharding import PartitionSpec as P

EPS = 1e-06
MASKED = -1e30


def normalize(row_block, gain):
    values = row_block.astype(jnp.float32)
    inverse = lax.rsqrt(jnp.mean(values * values, axis=-1, keepdims=True) + EPS)
    return values * inverse * gain


def on_device(
    mixer_input,
    forget_cumsum,
    mixer_gain,
    query_weight,
    key_weight,
    value_weight,
    out_weight,
    post_gain,
    expert_input,
    expert_gain,
    routes,
    route_weight,
    expert_gate,
    expert_upward,
    expert_down,
):
    ep_count = lax.axis_size("ep")
    tp_count = lax.axis_size("tp")
    mix_rows = mixer_input.shape[0]
    feature_width = mixer_input.shape[1]
    heads_local = forget_cumsum.shape[0]
    head_width = query_weight.shape[1]
    head_dim = head_width // heads_local
    group_span = mix_rows * tp_count
    first_pos = lax.axis_index("ep") * group_span
    last_pos = first_pos + group_span - 1
    score_scale = head_dim ** (-0.5)
    normed = normalize(mixer_input, mixer_gain).astype(jnp.bfloat16)
    segment = lax.all_gather(normed, "tp", axis=0, tiled=True)
    products = [
        jnp.dot(segment, weight, preferred_element_type=jnp.float32)
        for weight in (query_weight, key_weight, value_weight)
    ]
    joined = jnp.concatenate(products, axis=1).astype(jnp.bfloat16)
    queries = joined[:, :head_width].reshape(group_span, heads_local, head_dim)
    key_rows = joined[:, head_width : 2 * head_width]
    value_rows = joined[:, 2 * head_width :]
    query_pos = first_pos + jnp.arange(group_span, dtype=jnp.int32)
    query_gate = lax.dynamic_slice_in_dim(forget_cumsum, first_pos, group_span, 1)

    def key_block(state, key_part, value_part, key_first):
        key_count = key_part.shape[0]

        def compute(current):
            running_max, running_sum, running_acc = current
            key_heads = key_part.reshape(key_count, heads_local, head_dim)
            value_heads = value_part.reshape(key_count, heads_local, head_dim)
            key_gate = lax.dynamic_slice_in_dim(forget_cumsum, key_first, key_count, 1)
            scores = (
                jnp.einsum("qhd,khd->hqk", queries, key_heads, preferred_element_type=jnp.float32)
                * score_scale
            )
            scores = scores + query_gate[:, :, None] - key_gate[:, None, :]
            key_pos = key_first + jnp.arange(key_count, dtype=jnp.int32)
            visible = (key_pos[None, :] <= query_pos[:, None])[None]
            scores = jnp.where(visible, scores, MASKED)
            new_max = jnp.maximum(running_max, jnp.max(scores, axis=-1))
            weights = jnp.where(visible, jnp.exp(scores - new_max[..., None]), 0.0)
            rescale = jnp.exp(running_max - new_max)
            running_sum = running_sum * rescale + jnp.sum(weights, axis=-1)
            running_acc = running_acc * rescale[..., None] + jnp.einsum(
                "hqk,khd->hqd",
                weights.astype(jnp.bfloat16),
                value_heads,
                preferred_element_type=jnp.float32,
            )
            return (new_max, running_sum, running_acc)

        def keep_state(current):
            return current

        return lax.cond(key_first > last_pos, keep_state, compute, state)

    initial = (
        jnp.full((heads_local, group_span), MASKED, jnp.float32),
        jnp.zeros((heads_local, group_span), jnp.float32),
        jnp.zeros((heads_local, group_span, head_dim), jnp.float32),
    )
    key_part = lax.all_gather(key_rows, "ep", axis=0, tiled=True)
    value_part = lax.all_gather(value_rows, "ep", axis=0, tiled=True)
    row_count = key_part.shape[0]
    block_size = 512
    block_count = row_count // block_size

    def advance_increment(block_index, current):
        offset = block_index * block_size
        return key_block(
            current,
            lax.dynamic_slice_in_dim(key_part, offset, block_size, 0),
            lax.dynamic_slice_in_dim(value_part, offset, block_size, 0),
            offset,
        )

    running_max, running_sum, running_acc = lax.fori_loop(
        0, block_count, advance_increment, initial
    )
    attended = (running_acc / running_sum[..., None]).astype(jnp.bfloat16)
    attended = attended.transpose(1, 0, 2).reshape(group_span, head_width)
    moe_rows, top_count = routes.shape
    experts_local = expert_gate.shape[0]
    experts_all = ep_count * experts_local
    capacity = (moe_rows * top_count * 9 + 8 * experts_all - 1) // (8 * experts_all)
    slots_all = experts_all * capacity
    normed_moe = normalize(expert_input, expert_gain).astype(jnp.bfloat16)
    flat_routes = routes.reshape(-1)
    member = (flat_routes[:, None] == jnp.arange(experts_all, dtype=jnp.int32)[None, :]).astype(
        jnp.int32
    )
    before = jnp.cumsum(member, axis=0) - member
    slot_rank = jnp.sum(before * member, axis=1)
    slot_index = (flat_routes * capacity + slot_rank).reshape(moe_rows, top_count)
    slot_ids = jnp.arange(slots_all, dtype=jnp.int32)
    choosers = [
        (slot_index[:, which][:, None] == slot_ids[None, :]).astype(jnp.bfloat16)
        for which in range(top_count)
    ]
    dispatch = choosers[0]
    which = 1
    dispatch = dispatch + choosers[which]
    outgoing = lax.dot_general(
        dispatch, normed_moe, (((0,), (0,)), ((), ())), preferred_element_type=jnp.float32
    ).astype(jnp.bfloat16)
    outgoing = outgoing.reshape(ep_count, experts_local, capacity, feature_width)
    copies = jnp.broadcast_to(
        outgoing[:, None], (ep_count, tp_count, experts_local, capacity, feature_width)
    )
    copies = copies.reshape(ep_count * tp_count, experts_local, capacity, feature_width)
    stacked = lax.all_to_all(copies, ("ep", "tp"), split_axis=0, concat_axis=0, tiled=True).reshape(
        ep_count, tp_count, experts_local, capacity, feature_width
    )
    shard_axis = 1
    expert_rows_count = ep_count * experts_local * capacity

    def expert_term(block_index):
        selected = lax.dynamic_index_in_dim(stacked, block_index, shard_axis, keepdims=False)
        gate_proj = jnp.einsum(
            "secd,edf->secf", selected, expert_gate, preferred_element_type=jnp.float32
        )
        upward = jnp.einsum(
            "secd,edf->secf", selected, expert_upward, preferred_element_type=jnp.float32
        )
        hidden = (jax.nn.silu(gate_proj) * upward).astype(jnp.bfloat16)
        result = jnp.einsum(
            "secf,efd->secd", hidden, expert_down, preferred_element_type=jnp.float32
        )
        return result.reshape(expert_rows_count, feature_width)

    selected = attended
    mixer_sum = lax.psum_scatter(
        jnp.dot(selected, out_weight, preferred_element_type=jnp.float32).astype(jnp.bfloat16),
        "tp",
        scatter_dimension=0,
        tiled=True,
    ).astype(jnp.float32)
    first_block = jnp.int32(0) // expert_rows_count
    pieces = [
        expert_term(first_block + offset)
        for offset in range(expert_rows_count * lax.axis_size("tp") // expert_rows_count)
    ]
    expert_sum = lax.psum_scatter(
        jnp.concatenate(pieces, axis=0).astype(jnp.bfloat16), "tp", scatter_dimension=0, tiled=True
    )
    mixer_output = normalize(mixer_sum, post_gain).astype(jnp.bfloat16)
    results = expert_sum.reshape(ep_count, experts_local, capacity, feature_width)
    returned = lax.all_to_all(results, "ep", split_axis=0, concat_axis=0, tiled=True).reshape(
        slots_all, feature_width
    )
    combined = jnp.zeros((moe_rows, feature_width), jnp.float32)
    for which in range(top_count):
        picked = jnp.dot(choosers[which], returned, preferred_element_type=jnp.float32)
        combined = combined + route_weight[:, which : which + 1] * picked
    expert_output = combined.astype(jnp.bfloat16)
    return (mixer_output, expert_output)


def solution(mesh):
    in_specs = (
        P(("grp", "ep", "tp"), None),
        P("tp", "grp"),
        P(),
        P(None, "tp"),
        P(None, "tp"),
        P(None, "tp"),
        P("tp", None),
        P(),
        P(("grp", "ep", "tp"), None),
        P(),
        P(("grp", "ep", "tp"), None),
        P(("grp", "ep", "tp"), None),
        P("ep", None, "tp"),
        P("ep", None, "tp"),
        P("ep", "tp", None),
    )
    out_specs = (P(("grp", "ep", "tp"), None), P(("grp", "ep", "tp"), None))
    return jax.shard_map(
        on_device, mesh=mesh, in_specs=in_specs, out_specs=out_specs, check_vma=False
    )
```

profile of v0, /device:TPU:0, one launch (start us, length us, event | category | flops | bytes accessed | tf_op | source)
XLA Modules:
  0.0 285.0 jit_solution(11052232415735645723)
XLA Ops:
  7.2 0.0 copy-start
  7.2 0.9 copy.79
  8.1 0.1 eq.59
  8.3 0.1 eq.55
  8.4 1.2 reduce-window.6
  9.6 0.1 slice.40
  9.7 0.1 copy.81
  9.9 0.1 copy.82
  10.0 0.1 add_bitcast_fusion
  10.1 0.1 reduce_sum.53
  10.2 0.1 copy.83
  10.3 0.7 multiply_add_fusion.1
  11.0 1.2 fusion.97
  12.2 1.6 convolution_convert_fusion.1
  13.8 2.8 broadcast_in_dim.67
  16.6 7.6 %all-to-all-start = ((bf16[16,1,72,2048]{3,2,1,0:T(8,128)(2,1)}), bf16[16,1,72,2048]{3,2,1,0:T(8,128)(2,1)}, u32[]{:S(2)}, u32[]{:S(2)}) async-start(bf16[16,1,72,2048]{3,2,1,0:T(8,128)(2,1)} %bitcast.288), calls=%async_computation.1 | async-start | bytes 9437184 | tf_op jit(solution)/shard_map/all_to_all | solution.py:144
  24.2 0.0 all-gather.4.cloned.1.call-start
  24.2 0.2 fusion.91
  24.4 1.0 fusion.93
  25.4 0.0 all-gather.4.cloned.1.call-update
  25.5 0.0 all-gather.6.cloned.1.call-start
  25.5 48.1 %all-gather.4.cloned.1.call-done = bf16[512,2048]{1,0:T(8,128)(2,1)} async-done(((bf16[128,2048]{1,0:T(8,128)(2,1)}), bf16[512,2048]{1,0:T(8,128)(2,1)}) %all-gather.4.cloned.1.call-update) | async-done | bytes 2097168 | tf_op jit(solution)/shard_map/all_gather | solution.py:45
  73.6 3.3 %convolution_convert_fusion.8 = bf16[512,256]{1,0:T(8,128)(2,1)} fusion(bf16[512,2048]{1,0:T(8,128)(2,1)} %all-gather.4.cloned.1.call-done, bf16[2048,256]{1,0:T(8,128)(2,1)} %param.23), kind=kOutput, calls=%fused_computation.73 | convolution fusion | flops 537001984 | bytes 3407872 | tf_op jit(solution)/shard_map/dot_general | solution.py:47
  76.9 0.0 all-gather.6.cloned.1.call-update
  76.9 0.0 all-gather.8.cloned.1.call-start
  77.0 3.0 %convolution_convert_fusion.6 = bf16[512,256]{1,0:T(8,128)(2,1)} fusion(bf16[512,2048]{1,0:T(8,128)(2,1)} %all-gather.4.cloned.1.call-done, bf16[2048,256]{1,0:T(8,128)(2,1)S(1)} %copy-done.7), kind=kOutput, calls=%fused_computation.71 | convolution fusion | flops 537001984 | bytes 3407872 | tf_op jit(solution)/shard_map/dot_general | solution.py:47
  80.0 0.0 all-gather.8.cloned.1.call-update
  80.0 0.0 reduce-scatter.5.cloned.1.call-start
  80.1 47.6 %all-to-all-done = bf16[16,1,72,2048]{3,2,1,0:T(8,128)(2,1)} async-done(((bf16[16,1,72,2048]{3,2,1,0:T(8,128)(2,1)}), bf16[16,1,72,2048]{3,2,1,0:T(8,128)(2,1)}, u32[]{:S(2)}, u32[]{:S(2)}) %all-to-all-start) | async-done | bytes 4718624 | tf_op jit(solution)/shard_map/all_to_all | solution.py:144
  127.7 3.7 %fusion.31 = f32[4,1,72,512]{3,2,0,1:T(8,128)} fusion(bf16[1,2048,512]{2,1,0:T(8,128)(2,1)} %param.31, bf16[4,4,1,72,2048]{4,3,1,0,2:T(8,128)(2,1)} %bitcast.13), kind=kOutput, calls=%fused_computation.55 | convolution fusion | flops 603979776 | bytes 3866624 | tf_op jit(solution)/shard_map/secd,edf->secf/dot_general | solution.py:152
  131.4 2.9 %fusion.34 = f32[4,1,72,512]{3,2,0,1:T(8,128)} fusion(bf16[1,2048,512]{2,1,0:T(8,128)(2,1)S(1)} %copy-done.6, bf16[4,4,1,72,2048]{4,3,1,0,2:T(8,128)(2,1)} %bitcast.13), kind=kOutput, calls=%fused_computation.56 | convolution fusion | flops 603979776 | bytes 3866624 | tf_op jit(solution)/shard_map/secd,edf->secf/dot_general | solution.py:152
  134.3 2.9 %fusion.37 = f32[4,1,72,512]{3,2,0,1:T(8,128)} fusion(bf16[1,2048,512]{2,1,0:T(8,128)(2,1)S(1)} %copy-done.6, bf16[4,4,1,72,2048]{4,3,1,0,2:T(8,128)(2,1)} %bitcast.13), kind=kOutput, calls=%fused_computation.57 | convolution fusion | flops 603979776 | bytes 3866624 | tf_op jit(solution)/shard_map/secd,edf->secf/dot_general | solution.py:152
  137.1 3.6 %convolution_convert_fusion.5 = bf16[4,72,2048]{2,1,0:T(8,128)(2,1)S(1)} fusion(bf16[1,512,2048]{2,1,0:T(8,128)(2,1)S(1)} %copy-done, bf16[1,2048,512]{2,1,0:T(8,128)(2,1)} %param.32, bf16[4,4,1,72,2048]{4,3,1,0,2:T(8,128)(2,1)} %bitcast.13, f32[4,1,72,512]{3,2,0,1:T(8,128)} %fusion.31), kind=kOutput, calls=%fused_computation.24 | convolution fusion | flops 1209434112 | bytes 7143424 | tf_op jit(solution)/shard_map/secf,efd->secd/dot_general | solution.py:159
  140.8 4.6 %convolution_convert_fusion.4 = bf16[4,72,2048]{2,1,0:T(8,128)(2,1)} fusion(bf16[1,512,2048]{2,1,0:T(8,128)(2,1)S(1)} %copy-done, bf16[1,2048,512]{2,1,0:T(8,128)(2,1)} %param.32, bf16[4,4,1,72,2048]{4,3,1,0,2:T(8,128)(2,1)} %bitcast.13, f32[4,1,72,512]{3,2,0,1:T(8,128)} %fusion.34), kind=kOutput, calls=%fused_computation.23 | convolution fusion | flops 1209434112 | bytes 7143424 | tf_op jit(solution)/shard_map/secf,efd->secd/dot_general | solution.py:159
  145.4 4.6 %convolution_convert_fusion.3 = bf16[4,72,2048]{2,1,0:T(8,128)(2,1)} fusion(bf16[1,512,2048]{2,1,0:T(8,128)(2,1)S(1)} %copy-done, bf16[1,2048,512]{2,1,0:T(8,128)(2,1)} %param.32, bf16[4,4,1,72,2048]{4,3,1,0,2:T(8,128)(2,1)} %bitcast.13, f32[4,1,72,512]{3,2,0,1:T(8,128)} %fusion.37), kind=kOutput, calls=%fused_computation.22 | convolution fusion | flops 1209434112 | bytes 7143424 | tf_op jit(solution)/shard_map/secf,efd->secd/dot_general | solution.py:159
  150.0 3.6 %fusion.40 = f32[4,1,72,512]{3,2,0,1:T(8,128)} fusion(bf16[1,2048,512]{2,1,0:T(8,128)(2,1)} %param.31, bf16[4,4,1,72,2048]{4,3,1,0,2:T(8,128)(2,1)} %bitcast.13), kind=kOutput, calls=%fused_computation.58 | convolution fusion | flops 603979776 | bytes 3866624 | tf_op jit(solution)/shard_map/secd,edf->secf/dot_general | solution.py:152
  153.6 4.6 %convolution_convert_fusion.2 = bf16[4,72,2048]{2,1,0:T(8,128)(2,1)} fusion(bf16[1,512,2048]{2,1,0:T(8,128)(2,1)S(1)} %copy-done, bf16[1,2048,512]{2,1,0:T(8,128)(2,1)} %param.32, bf16[4,4,1,72,2048]{4,3,1,0,2:T(8,128)(2,1)} %bitcast.13, f32[4,1,72,512]{3,2,0,1:T(8,128)} %fusion.40), kind=kOutput, calls=%fused_computation.21 | convolution fusion | flops 1209434112 | bytes 7143424 | tf_op jit(solution)/shard_map/secf,efd->secd/dot_general | solution.py:159
  158.2 3.9 %pad_maximum_fusion = bf16[1152,2048]{1,0:T(8,128)(2,1)} fusion(bf16[288,2048]{1,0:T(8,128)(2,1)} %bitcast.297, bf16[288,2048]{1,0:T(8,128)(2,1)} %bitcast.296, bf16[288,2048]{1,0:T(8,128)(2,1)} %bitcast.295, bf16[288,2048]{1,0:T(8,128)(2,1)S(1)} %bitcast.294), kind=kLoop, calls=%fused_computation.18 | loop fusion | flops 18874368 | bytes 9437184 | tf_op jit(solution)/shard_map/concatenate | solution.py:177
  162.1 0.0 reduce-scatter.5.cloned.1.call-update
  162.1 0.2 reduce-scatter.3.cloned.1.call-start
  162.3 0.5 copy-done.2
  162.8 2.6 convolution_convert_fusion.7
  165.4 0.2 copy.76
  165.6 0.0 all-gather.6.cloned.1.call-done
  165.6 2.3 copy.75
  167.9 2.3 copy.77
  170.2 3.8 %while.18 = (s32[]{:T(128)}, f32[2,512]{1,0:T(2,128)S(1)}, f32[2,512]{1,0:T(2,128)S(1)}, f32[2,512,128]{2,1,0:T(8,128)S(1)}, s32[]{:T(128)}, /*index=5*/bf16[204...) while((s32[]{:T(128)}, f32[2,512]{1,0:T(2,128)S(1)}, ...), condition=%wide.region_6.7_spmd.clone, body=%wide.region_1.6_spmd.clone.sunk | while | flops 274729984 | bytes 10318161 | solution.py:110
  170.3 3.5 %conditional.3 = (f32[2,512]{1,0:T(2,128)S(1)}, f32[2,512]{1,0:T(2,128)S(1)}, f32[2,512,128]{2,1,0:T(8,128)S(1)}) conditional(s32[]{:T(128)} %convert_element_type.155, (s32[]{:T(128)}, s32[]{:T(128)}, bf16[2048,256]{0,1:T(8,128)(2,1)}, bf16[512,2,128]{2,0,1:T(8,128)(2,1)S(1)}, f32[2,512]{1,0:T(2,128)S(1)}, /*index=5*/f32[2,2048]{1,0:T(2,128)S(1)}, ...), branch_computations={%region_2.4_spmd, %region_5.5_spmd} | conditional | flops 274729984 | bytes 10307658 | solution.py:88
  170.3 1.1 constant_dynamic-slice_fusion.1
  171.4 0.2 broadcast_compare_fusion
  171.6 0.8 fusion.151
  172.4 0.4 fusion.3
  172.9 0.9 convolution_add_fusion
  174.1 0.2 copy.78
  174.3 0.1 divide_convert_fusion
  174.3 3.4 %convolution_convert_fusion = bf16[512,2048]{1,0:T(8,128)(2,1)} fusion(bf16[512,256]{0,1:T(8,128)(2,1)S(1)} %bitcast.293, bf16[256,2048]{1,0:T(8,128)(2,1)} %param.25), kind=kOutput, calls=%fused_computation.19 | convolution fusion | flops 537919488 | bytes 3407872 | tf_op jit(solution)/shard_map/dot_general | solution.py:166
  177.7 0.0 reduce-scatter.3.cloned.1.call-update
  177.7 62.1 %reduce-scatter.5.cloned.1.call-done = bf16[288,2048]{1,0:T(8,128)(2,1)} async-done(((bf16[1152,2048]{1,0:T(8,128)(2,1)}), bf16[288,2048]{1,0:T(8,128)(2,1)}) %reduce-scatter.5.cloned.1.call-update) | async-done | bytes 1179664 | tf_op jit(solution)/shard_map/reduce_scatter | solution.py:176
  239.8 4.6 %all-to-all-start.1 = ((bf16[4,1,72,2048]{3,2,1,0:T(8,128)(2,1)}), bf16[4,1,72,2048]{3,2,1,0:T(8,128)(2,1)S(1)}, u32[]{:S(2)}, u32[]{:S(2)}) async-start(bf16[4,1,72,2048]{3,2,1,0:T(8,128)(2,1)} %bitcast.298), calls=%async_computation.3 | async-start | bytes 2359296 | tf_op jit(solution)/shard_map/all_to_all | solution.py:181
  244.4 28.9 %reduce-scatter.3.cloned.1.call-done = bf16[128,2048]{1,0:T(8,128)(2,1)} async-done(((bf16[512,2048]{1,0:T(8,128)(2,1)}), bf16[128,2048]{1,0:T(8,128)(2,1)}) %reduce-scatter.3.cloned.1.call-update) | async-done | bytes 524304 | tf_op jit(solution)/shard_map/reduce_scatter | solution.py:165
  273.4 1.2 fusion.94
  274.6 2.0 fusion.96
  276.7 0.5 convolution_multiply_fusion.1
  277.1 1.3 fusion.10
  (47 shorter events, 0.3 us)
Async XLA Ops:
  7.2 130.0 %copy-start = (bf16[1,512,2048]{2,1,0:T(8,128)(2,1)S(1)}, bf16[1,512,2048]{2,1,0:T(8,128)(2,1)}, u32[]{:S(2)}) copy-start(bf16[1,512,2048]{2,1,0:T(8,128)(2,1)} %param.33) | copy-start | bytes 6291460
  16.6 7.6 %copy-start.1 = (bf16[128,2048]{1,0:T(8,128)(2,1)S(1)}, bf16[128,2048]{1,0:T(8,128)(2,1)}, u32[]{:S(2)}) copy-start(bf16[128,2048]{1,0:T(8,128)(2,1)} %param.19) | copy-start | bytes 1572868
  16.6 7.8 %copy-start.3 = (f32[2048]{0:T(1024)S(1)}, f32[2048]{0:T(1024)}, u32[]{:S(2)}) copy-start(f32[2048]{0:T(1024)} %param.21) | copy-start | bytes 24580
  16.6 111.1 %all-to-all-start = ((bf16[16,1,72,2048]{3,2,1,0:T(8,128)(2,1)}), bf16[16,1,72,2048]{3,2,1,0:T(8,128)(2,1)}, u32[]{:S(2)}, u32[]{:S(2)}) async-start(bf16[16,1,72,2048]{3,2,1,0:T(8,128)(2,1)} %bitcast.288), calls=%async_computation.1 | async-start | bytes 9437184 | tf_op jit(solution)/shard_map/all_to_all | solution.py:144
  24.2 49.5 %all-gather.4.cloned.1.call-start = ((), (), s32[]{:S(2)}) async-start(), calls=%async_computation.4 | async-start | bytes 2621440 | tf_op jit(solution)/shard_map/all_gather | solution.py:45
  25.4 51.5 %copy-start.7 = (bf16[2048,256]{1,0:T(8,128)(2,1)S(1)}, bf16[2048,256]{1,0:T(8,128)(2,1)}, u32[]{:S(2)}) copy-start(bf16[2048,256]{1,0:T(8,128)(2,1)} %param.24) | copy-start | bytes 3145732
  25.5 140.1 %all-gather.6.cloned.1.call-start = ((), (), s32[]{:S(2)}) async-start(), calls=%async_computation.5 | async-start | bytes 1310720 | tf_op jit(solution)/shard_map/all_gather | solution.py:95
  76.9 91.0 %all-gather.8.cloned.1.call-start = ((), (), s32[]{:S(2)}) async-start(), calls=%async_computation.6 | async-start | bytes 1310720 | tf_op jit(solution)/shard_map/all_gather | solution.py:96
  80.0 159.8 %reduce-scatter.5.cloned.1.call-start = ((), (), s32[]{:S(2)}) async-start(), calls=%async_computation.8 | async-start | bytes 5898240 | tf_op jit(solution)/shard_map/reduce_scatter | solution.py:176
  127.7 3.7 %copy-start.6 = (bf16[1,2048,512]{2,1,0:T(8,128)(2,1)S(1)}, bf16[1,2048,512]{2,1,0:T(8,128)(2,1)}, u32[]{:S(2)}) copy-start(bf16[1,2048,512]{2,1,0:T(8,128)(2,1)} %param.31) | copy-start | bytes 6291460
  162.1 0.7 copy-start.2
  162.1 111.3 %reduce-scatter.3.cloned.1.call-start = ((), (), s32[]{:S(2)}) async-start(), calls=%async_computation.7 | async-start | bytes 2621440 | tf_op jit(solution)/shard_map/reduce_scatter | solution.py:165
  177.7 66.7 %copy-start.5 = (f32[128,2]{0,1:T(2,128)S(1)}, f32[128,2]{0,1:T(2,128)}, u32[]{:S(2)}) copy-start(f32[128,2]{0,1:T(2,128)} %param.30) | copy-start | bytes 3076
  177.7 96.9 %copy-start.4 = (f32[2048]{0:T(1024)S(1)}, f32[2048]{0:T(1024)}, u32[]{:S(2)}) copy-start(f32[2048]{0:T(1024)} %param.26) | copy-start | bytes 24580
  239.8 36.8 %all-to-all-start.1 = ((bf16[4,1,72,2048]{3,2,1,0:T(8,128)(2,1)}), bf16[4,1,72,2048]{3,2,1,0:T(8,128)(2,1)S(1)}, u32[]{:S(2)}, u32[]{:S(2)}) async-start(bf16[4,1,72,2048]{3,2,1,0:T(8,128)(2,1)} %bitcast.298), calls=%async_computation.3 | async-start | bytes 2359296 | tf_op jit(solution)/shard_map/all_to_all | solution.py:181
Sparse Core Ops, SparseCore 0:
  27.1 46.4 all-gather.3
  77.0 41.1 all-gather.5
  120.4 43.0 all-gather.7
  165.9 73.9 reduce-scatter.4
  242.2 31.1 reduce-scatter.2
where the time goes:
time: 286 us; the launch traced here: 285 us
  waiting for transfers between devices  187 us (65%)
  matrix products  47.8 us (17%)
  between operations  14 us (5%)
  starting transfers between devices  12.6 us (4%)
  other arithmetic  12.3 us (4%)
  local copies, waits for them, and re-layouts  11 us (4%)
    reduce_scatter x1, waiting for transfers between devices, on_device(): lax.psum_scatter(jnp.concatenate(pieces, axis=0).astype(jnp.bfloat16), 't...  62.1 us
    all_gather x1, waiting for transfers between devices, on_device(): segment = lax.all_gather(normed, 'tp', axis=0, tiled=True)  48.1 us
    all_to_all x1, waiting for transfers between devices, on_device(): lax.all_to_all(copies, ('ep', 'tp'), split_axis=0, concat_axis=0, tiled=T...  47.6 us
    reduce_scatter x1, waiting for transfers between devices, on_device(): lax.psum_scatter(jnp.dot(selected, out_weight, preferred_element_type=jnp...  28.9 us
    dot_general x4, matrix products, expert_term(): jnp.einsum('secf,efd->secd', hidden, expert_down, preferred_element_type=...  17.4 us
    dot_general x4, matrix products, expert_term(): jnp.einsum('secd,edf->secf', selected, expert_gate, preferred_element_typ...  13 us
    dot_general x3, matrix products, on_device(): jnp.dot(segment, weight, preferred_element_type=jnp.float32)  8.88 us
    all_to_all x1, starting transfers between devices, on_device(): lax.all_to_all(copies, ('ep', 'tp'), split_axis=0, concat_axis=0, tiled=T...  7.56 us
  transfers between devices with their start and end apart: 7, of which 4 were waited for; matrix products, arithmetic and copies ran while one was open for 21% of the time, Pallas kernels for 0%

commit v1 on v0

--- a/solution.py
+++ b/solution.py
@@ -1,10 +1,32 @@
+import functools
 import jax
 import jax.numpy as jnp
 from jax import lax
 from jax.sharding import PartitionSpec as P
+from jax.lax import axis_index, axis_size, ppermute
 
 EPS = 1e-06
 MASKED = -1e30
+
+
+def joints_treat(inner_x, axis_name):
+    axis_len = axis_size(axis_name)
+    pool = []
+    for b in range(axis_len):
+        pool.append((b, (b + 1) % axis_len))
+
+    def assign_heaps_up(carry_in):
+        if len(carry_in) == axis_len:
+            return carry_in
+        r1 = ppermute(carry_in[0], axis_name, pool)
+        return assign_heaps_up([r1, *carry_in])
+
+    outer = assign_heaps_up([inner_x])
+    plain = jnp.concatenate(outer, axis=0)
+    return jnp.roll(plain, (axis_index(axis_name) + 1) * inner_x.shape[0], axis=0)
+
+
+choose_pools_by_axis = functools.partial(joints_treat, axis_name="tp")
 
 
 def normalize(row_block, gain):
@@ -42,7 +64,7 @@
     last_pos = first_pos + group_span - 1
     score_scale = head_dim ** (-0.5)
     normed = normalize(mixer_input, mixer_gain).astype(jnp.bfloat16)
-    segment = lax.all_gather(normed, "tp", axis=0, tiled=True)
+    segment = choose_pools_by_axis(normed)
     products = [
         jnp.dot(segment, weight, preferred_element_type=jnp.float32)
         for weight in (query_weight, key_weight, value_weight)

time: 286 us -> 275 us (0.962)
  waiting for transfers between devices: 187 us -> 170 us
  local copies, waits for them, and re-layouts: 11 us -> 17.6 us
    ppermute x0 -> x3, waiting for transfers between devices: none -> 59.5 us  [assign_heaps_up(): r1 = ppermute(carry_in[0], axis_name, pool)]
    all_gather x1 -> x0, waiting for transfers between devices: 48.1 us -> none  [on_device(): segment = lax.all_gather(normed, 'tp', axis=0, tiled=True)]
    all_to_all x1, waiting for transfers between devices: 47.6 us -> 14.9 us  [on_device(): lax.all_to_all(copies, ('ep', 'tp'), split_axis=0, concat_axis=0, tiled=T...]
    all_gather x1, waiting for transfers between devices: 0.02 us -> 13.6 us  [on_device(): key_part = lax.all_gather(key_rows, 'ep', axis=0, tiled=True)]
    reduce_scatter x1, waiting for transfers between devices: 62.1 us -> 52.7 us  [on_device(): lax.psum_scatter(jnp.concatenate(pieces, axis=0).astype(jnp.bfloat16), 't...]
    unnamed x20 -> x30, local copies, waits for them, and re-layouts: 6.17 us -> 12.7 us
  transfers between devices with their start and end apart: 7 -> 9, of which waited for: 4 -> 7; matrix products, arithmetic and copies ran while one was open for 21% -> 23% of each run, Pallas kernels for 0% -> 0%
where the time goes in v1:
time: 275 us; the launch traced here: 274 us
  waiting for transfers between devices  170 us (62%)
  matrix products  45.9 us (17%)
  local copies, waits for them, and re-layouts  17.6 us (6%)
  between operations  15.7 us (6%)
  starting transfers between devices  12.9 us (5%)
  other arithmetic  12 us (4%)
    ppermute x3, waiting for transfers between devices, assign_heaps_up(): r1 = ppermute(carry_in[0], axis_name, pool)  59.5 us
    reduce_scatter x1, waiting for transfers between devices, on_device(): lax.psum_scatter(jnp.concatenate(pieces, axis=0).astype(jnp.bfloat16), 't...  52.7 us
    reduce_scatter x1, waiting for transfers between devices, on_device(): lax.psum_scatter(jnp.dot(selected, out_weight, preferred_element_type=jnp...  28.9 us
    dot_general x4, matrix products, expert_term(): jnp.einsum('secf,efd->secd', hidden, expert_down, preferred_element_type=...  17.4 us
    all_to_all x1, waiting for transfers between devices, on_device(): lax.all_to_all(copies, ('ep', 'tp'), split_axis=0, concat_axis=0, tiled=T...  14.9 us
    all_gather x1, waiting for transfers between devices, on_device(): key_part = lax.all_gather(key_rows, 'ep', axis=0, tiled=True)  13.6 us
    dot_general x4, matrix products, expert_term(): jnp.einsum('secd,edf->secf', selected, expert_gate, preferred_element_typ...  13 us
    unnamed x30, local copies, waits for them, and re-layouts  12.7 us
  transfers between devices with their start and end apart: 9, of which 7 were waited for; matrix products, arithmetic and copies ran while one was open for 23% of the time, Pallas kernels for 0%

profile of v1, /device:TPU:0, one launch (start us, length us, event | category | flops | bytes accessed | tf_op | source)
XLA Modules:
  0.0 274.1 jit_solution(2790966671490310777)
XLA Ops:
  8.0 0.9 copy.79
  8.9 0.1 eq.62
  9.1 0.1 eq.58
  9.2 1.2 reduce-window.6
  10.5 0.1 slice.40
  10.5 0.1 copy.81
  10.7 0.1 copy.82
  10.8 0.1 add_bitcast_fusion
  10.9 0.1 reduce_sum.53
  11.0 0.1 copy.83
  11.1 0.7 multiply_add_fusion.1
  11.8 1.2 fusion.112
  13.0 1.6 convolution_convert_fusion.1
  14.7 2.8 %broadcast_in_dim.67 = bf16[4,4,72,2048]{3,2,1,0:T(8,128)(2,1)} broadcast(bf16[4,72,2048]{2,1,0:T(8,128)(2,1)S(1)} %bitcast.289), dimensions={0,2,3} | broadcast | bytes 5898240 | tf_op jit(solution)/shard_map/broadcast_in_dim | solution.py:162
  17.4 7.6 %all-to-all-start = ((bf16[16,1,72,2048]{3,2,1,0:T(8,128)(2,1)}), bf16[16,1,72,2048]{3,2,1,0:T(8,128)(2,1)}, u32[]{:S(2)}, u32[]{:S(2)}) async-start(bf16[16,1,72,2048]{3,2,1,0:T(8,128)(2,1)} %bitcast.285), calls=%async_computation.1 | async-start | bytes 9437184 | tf_op jit(solution)/shard_map/all_to_all | solution.py:166
  25.1 0.2 fusion.106
  25.3 0.2 fusion.108
  25.5 0.4 collective-permute-start
  25.9 34.1 %collective-permute-done = bf16[128,2048]{1,0:T(8,128)(2,1)S(1)} collective-permute-done((bf16[128,2048]{1,0:T(8,128)(2,1)S(1)}, bf16[128,2048]{1,0:T(8,128)(2,1)S(1)}, u32[]{:S(2)}, u32[]{:S(2)}) %collective-permute-start) | collective-permute-done | bytes 524320 | tf_op jit(solution)/shard_map/ppermute | solution.py:21
  60.0 14.8 %collective-permute-done.1 = bf16[128,2048]{1,0:T(8,128)(2,1)} collective-permute-done((bf16[128,2048]{1,0:T(8,128)(2,1)S(1)}, bf16[128,2048]{1,0:T(8,128)(2,1)}, u32[]{:S(2)}, u32[]{:S(2)}) %collective-permute-start.1) | collective-permute-done | bytes 524320 | tf_op jit(solution)/shard_map/ppermute | solution.py:21
  74.8 10.6 %collective-permute-done.2 = bf16[128,2048]{1,0:T(8,128)(2,1)} collective-permute-done((bf16[128,2048]{1,0:T(8,128)(2,1)}, bf16[128,2048]{1,0:T(8,128)(2,1)}, u32[]{:S(2)}, u32[]{:S(2)}) %collective-permute-start.2) | collective-permute-done | bytes 524320 | tf_op jit(solution)/shard_map/ppermute | solution.py:21
  85.4 1.1 constant_dynamic-update-slice_fusion.7
  86.5 1.1 constant_dynamic-update-slice_fusion.6
  87.6 0.2 constant_dynamic-update-slice_fusion.4
  87.8 1.2 constant_dynamic-update-slice_fusion.3
  89.0 1.1 constant_dynamic-update-slice_fusion.2
  90.1 0.2 constant_dynamic-update-slice_fusion
  90.3 2.1 copy-done.3
  92.4 1.4 fusion.91
  93.9 3.0 %fusion.85 = bf16[512,256]{1,0:T(8,128)(2,1)} fusion(bf16[2048,256]{1,0:T(8,128)(2,1)S(1)} %copy-done.9, bf16[1024,2048]{1,0:T(8,128)(2,1)} %copy-done.3, s32[]{:T(128)S(6)} %select_n.53), kind=kOutput, calls=%fused_computation.77 | convolution fusion | flops 537001984 | bytes 3407876 | tf_op jit(solution)/shard_map/dot_general | solution.py:69
  97.0 14.9 %all-to-all-done = bf16[16,1,72,2048]{3,2,1,0:T(8,128)(2,1)} async-done(((bf16[16,1,72,2048]{3,2,1,0:T(8,128)(2,1)}), bf16[16,1,72,2048]{3,2,1,0:T(8,128)(2,1)}, u32[]{:S(2)}, u32[]{:S(2)}) %all-to-all-start) | async-done | bytes 4718624 | tf_op jit(solution)/shard_map/all_to_all | solution.py:166
  111.8 3.7 %fusion.37 = f32[4,1,72,512]{3,2,0,1:T(8,128)} fusion(bf16[1,2048,512]{2,1,0:T(8,128)(2,1)} %param.31, bf16[4,4,1,72,2048]{4,3,1,0,2:T(8,128)(2,1)} %bitcast.13), kind=kOutput, calls=%fused_computation.61 | convolution fusion | flops 603979776 | bytes 3866624 | tf_op jit(solution)/shard_map/secd,edf->secf/dot_general | solution.py:174
  115.5 2.9 %fusion.40 = f32[4,1,72,512]{3,2,0,1:T(8,128)} fusion(bf16[1,2048,512]{2,1,0:T(8,128)(2,1)S(1)} %copy-done.7, bf16[4,4,1,72,2048]{4,3,1,0,2:T(8,128)(2,1)} %bitcast.13), kind=kOutput, calls=%fused_computation.62 | convolution fusion | flops 603979776 | bytes 3866624 | tf_op jit(solution)/shard_map/secd,edf->secf/dot_general | solution.py:174
  118.4 2.9 %fusion.43 = f32[4,1,72,512]{3,2,0,1:T(8,128)} fusion(bf16[1,2048,512]{2,1,0:T(8,128)(2,1)S(1)} %copy-done.7, bf16[4,4,1,72,2048]{4,3,1,0,2:T(8,128)(2,1)} %bitcast.13), kind=kOutput, calls=%fused_computation.63 | convolution fusion | flops 603979776 | bytes 3866624 | tf_op jit(solution)/shard_map/secd,edf->secf/dot_general | solution.py:174
  121.3 3.6 %convolution_convert_fusion.5 = bf16[4,72,2048]{2,1,0:T(8,128)(2,1)S(1)} fusion(bf16[1,512,2048]{2,1,0:T(8,128)(2,1)S(1)} %copy-done, bf16[1,2048,512]{2,1,0:T(8,128)(2,1)} %param.32, bf16[4,4,1,72,2048]{4,3,1,0,2:T(8,128)(2,1)} %bitcast.13, f32[4,1,72,512]{3,2,0,1:T(8,128)} %fusion.37), kind=kOutput, calls=%fused_computation.24 | convolution fusion | flops 1209434112 | bytes 7143424 | tf_op jit(solution)/shard_map/secf,efd->secd/dot_general | solution.py:181
  124.8 4.6 %convolution_convert_fusion.4 = bf16[4,72,2048]{2,1,0:T(8,128)(2,1)} fusion(bf16[1,512,2048]{2,1,0:T(8,128)(2,1)S(1)} %copy-done, bf16[1,2048,512]{2,1,0:T(8,128)(2,1)} %param.32, bf16[4,4,1,72,2048]{4,3,1,0,2:T(8,128)(2,1)} %bitcast.13, f32[4,1,72,512]{3,2,0,1:T(8,128)} %fusion.40), kind=kOutput, calls=%fused_computation.23 | convolution fusion | flops 1209434112 | bytes 7143424 | tf_op jit(solution)/shard_map/secf,efd->secd/dot_general | solution.py:181
  129.5 4.6 %convolution_convert_fusion.3 = bf16[4,72,2048]{2,1,0:T(8,128)(2,1)} fusion(bf16[1,512,2048]{2,1,0:T(8,128)(2,1)S(1)} %copy-done, bf16[1,2048,512]{2,1,0:T(8,128)(2,1)} %param.32, bf16[4,4,1,72,2048]{4,3,1,0,2:T(8,128)(2,1)} %bitcast.13, f32[4,1,72,512]{3,2,0,1:T(8,128)} %fusion.43), kind=kOutput, calls=%fused_computation.22 | convolution fusion | flops 1209434112 | bytes 7143424 | tf_op jit(solution)/shard_map/secf,efd->secd/dot_general | solution.py:181
  134.1 3.6 %fusion.46 = f32[4,1,72,512]{3,2,0,1:T(8,128)} fusion(bf16[1,2048,512]{2,1,0:T(8,128)(2,1)} %param.31, bf16[4,4,1,72,2048]{4,3,1,0,2:T(8,128)(2,1)} %bitcast.13), kind=kOutput, calls=%fused_computation.64 | convolution fusion | flops 603979776 | bytes 3866624 | tf_op jit(solution)/shard_map/secd,edf->secf/dot_general | solution.py:174
  137.7 4.6 %convolution_convert_fusion.2 = bf16[4,72,2048]{2,1,0:T(8,128)(2,1)} fusion(bf16[1,512,2048]{2,1,0:T(8,128)(2,1)S(1)} %copy-done, bf16[1,2048,512]{2,1,0:T(8,128)(2,1)} %param.32, bf16[4,4,1,72,2048]{4,3,1,0,2:T(8,128)(2,1)} %bitcast.13, f32[4,1,72,512]{3,2,0,1:T(8,128)} %fusion.46), kind=kOutput, calls=%fused_computation.21 | convolution fusion | flops 1209434112 | bytes 7143424 | tf_op jit(solution)/shard_map/secf,efd->secd/dot_general | solution.py:181
  142.2 3.9 %pad_maximum_fusion = bf16[1152,2048]{1,0:T(8,128)(2,1)} fusion(bf16[288,2048]{1,0:T(8,128)(2,1)} %bitcast.294, bf16[288,2048]{1,0:T(8,128)(2,1)} %bitcast.293, bf16[288,2048]{1,0:T(8,128)(2,1)} %bitcast.292, bf16[288,2048]{1,0:T(8,128)(2,1)S(1)} %bitcast.291), kind=kLoop, calls=%fused_computation.18 | loop fusion | flops 18874368 | bytes 9437184 | tf_op jit(solution)/shard_map/concatenate | solution.py:199
  146.2 0.2 reduce-scatter.3.cloned.1.call-start
  146.4 0.5 copy-done.4
  146.9 2.6 fusion.88
  149.5 0.2 copy.76
  149.7 2.3 copy.77
  152.0 13.6 %all-gather.3.cloned.1.call-done = bf16[2048,256]{1,0:T(8,128)(2,1)} async-done(((bf16[512,256]{1,0:T(8,128)(2,1)}), bf16[2048,256]{1,0:T(8,128)(2,1)}) %all-gather.3.cloned.1.call-update) | async-done | bytes 1048592 | tf_op jit(solution)/shard_map/all_gather | solution.py:117
  165.5 2.3 copy.75
  167.9 3.8 %while.18 = (s32[]{:T(128)}, f32[2,512]{1,0:T(2,128)S(1)}, f32[2,512]{1,0:T(2,128)S(1)}, f32[2,512,128]{2,1,0:T(8,128)S(1)}, s32[]{:T(128)}, /*index=5*/bf16[204...) while((s32[]{:T(128)}, f32[2,512]{1,0:T(2,128)S(1)}, ...), condition=%wide.region_6.7_spmd.clone, body=%wide.region_1.6_spmd.clone.sunk | while | flops 274729984 | bytes 10318161 | solution.py:132
  167.9 3.5 %conditional.3 = (f32[2,512]{1,0:T(2,128)S(1)}, f32[2,512]{1,0:T(2,128)S(1)}, f32[2,512,128]{2,1,0:T(8,128)S(1)}) conditional(s32[]{:T(128)} %convert_element_type.163, (s32[]{:T(128)}, s32[]{:T(128)}, bf16[2048,256]{0,1:T(8,128)(2,1)}, bf16[512,2,128]{2,0,1:T(8,128)(2,1)S(1)}, f32[2,512]{1,0:T(2,128)S(1)}, /*index=5*/f32[2,2048]{1,0:T(2,128)S(1)}, ...), branch_computations={%region_2.4_spmd, %region_5.5_spmd} | conditional | flops 274729984 | bytes 10307658 | solution.py:110
  167.9 1.1 constant_dynamic-slice_fusion.1
  169.0 0.2 broadcast_compare_fusion
  169.3 0.8 fusion.169
  170.1 0.4 fusion.3
  170.5 0.9 convolution_add_fusion
  171.7 0.2 copy.78
  171.9 0.1 divide_convert_fusion
  172.0 3.4 %convolution_convert_fusion = bf16[512,2048]{1,0:T(8,128)(2,1)} fusion(bf16[512,256]{0,1:T(8,128)(2,1)S(1)} %bitcast.290, bf16[256,2048]{1,0:T(8,128)(2,1)} %param.25), kind=kOutput, calls=%fused_computation.19 | convolution fusion | flops 537919488 | bytes 3407872 | tf_op jit(solution)/shard_map/dot_general | solution.py:188
  175.4 52.7 %reduce-scatter.5.cloned.1.call-done = bf16[288,2048]{1,0:T(8,128)(2,1)} async-done(((bf16[1152,2048]{1,0:T(8,128)(2,1)}), bf16[288,2048]{1,0:T(8,128)(2,1)}) %reduce-scatter.5.cloned.1.call-update) | async-done | bytes 1179664 | tf_op jit(solution)/shard_map/reduce_scatter | solution.py:198
  228.0 4.6 %all-to-all-start.1 = ((bf16[4,1,72,2048]{3,2,1,0:T(8,128)(2,1)}), bf16[4,1,72,2048]{3,2,1,0:T(8,128)(2,1)S(1)}, u32[]{:S(2)}, u32[]{:S(2)}) async-start(bf16[4,1,72,2048]{3,2,1,0:T(8,128)(2,1)} %bitcast.295), calls=%async_computation.3 | async-start | bytes 2359296 | tf_op jit(solution)/shard_map/all_to_all | solution.py:203
  232.7 28.9 %reduce-scatter.3.cloned.1.call-done = bf16[128,2048]{1,0:T(8,128)(2,1)} async-done(((bf16[512,2048]{1,0:T(8,128)(2,1)}), bf16[128,2048]{1,0:T(8,128)(2,1)}) %reduce-scatter.3.cloned.1.call-update) | async-done | bytes 524304 | tf_op jit(solution)/shard_map/reduce_scatter | solution.py:187
  261.6 1.2 fusion.109
  262.8 2.0 fusion.111
  264.8 0.5 convolution_multiply_fusion.1
  265.3 1.3 fusion.10
  (62 shorter events, 0.7 us)
Async XLA Ops:
  8.0 113.3 %copy-start = (bf16[1,512,2048]{2,1,0:T(8,128)(2,1)S(1)}, bf16[1,512,2048]{2,1,0:T(8,128)(2,1)}, u32[]{:S(2)}) copy-start(bf16[1,512,2048]{2,1,0:T(8,128)(2,1)} %param.33) | copy-start | bytes 6291460
  17.4 7.6 %copy-start.1 = (bf16[128,2048]{1,0:T(8,128)(2,1)S(1)}, bf16[128,2048]{1,0:T(8,128)(2,1)}, u32[]{:S(2)}) copy-start(bf16[128,2048]{1,0:T(8,128)(2,1)} %param.19) | copy-start | bytes 1572868
  17.4 7.8 %copy-start.2 = (f32[2048]{0:T(1024)S(1)}, f32[2048]{0:T(1024)}, u32[]{:S(2)}) copy-start(f32[2048]{0:T(1024)} %param.21) | copy-start | bytes 24580
  17.4 94.4 %all-to-all-start = ((bf16[16,1,72,2048]{3,2,1,0:T(8,128)(2,1)}), bf16[16,1,72,2048]{3,2,1,0:T(8,128)(2,1)}, u32[]{:S(2)}, u32[]{:S(2)}) async-start(bf16[16,1,72,2048]{3,2,1,0:T(8,128)(2,1)} %bitcast.285), calls=%async_computation.1 | async-start | bytes 9437184 | tf_op jit(solution)/shard_map/all_to_all | solution.py:166
  25.0 124.7 %all-gather.5.cloned.1.call-start = ((), (), s32[]{:S(2)}) async-start(), calls=%async_computation.5 | async-start | bytes 1310720 | tf_op jit(solution)/shard_map/all_gather | solution.py:118
  25.5 34.5 %collective-permute-start = (bf16[128,2048]{1,0:T(8,128)(2,1)S(1)}, bf16[128,2048]{1,0:T(8,128)(2,1)S(1)}, u32[]{:S(2)}, u32[]{:S(2)}) collective-permute-start(bf16[128,2048]{1,0:T(8,128)(2,1)S(1)} %fusion.108), channel_id=1, source_target_pairs={{0,1},{1,2},{2,3},{3,0},{4,5},{5,6},{6,7},{7,4},{8,9},{9,10},{10,1... | collective-permute-start | bytes 1572872 | tf_op jit(solution)/shard_map/ppermute | solution.py:21
  60.0 14.8 %collective-permute-start.1 = (bf16[128,2048]{1,0:T(8,128)(2,1)S(1)}, bf16[128,2048]{1,0:T(8,128)(2,1)}, u32[]{:S(2)}, u32[]{:S(2)}) collective-permute-start(bf16[128,2048]{1,0:T(8,128)(2,1)S(1)} %collective-permute-done), channel_id=1, source_target_pairs={{0,1},{1,2},{2,3},{3,0},{4,5},{5,6},{6,7},{7,4},{8,9},{9,10},{10,1... | collective-permute-start | bytes 1572872 | tf_op jit(solution)/shard_map/ppermute | solution.py:21
  74.7 10.6 %collective-permute-start.2 = (bf16[128,2048]{1,0:T(8,128)(2,1)}, bf16[128,2048]{1,0:T(8,128)(2,1)}, u32[]{:S(2)}, u32[]{:S(2)}) collective-permute-start(bf16[128,2048]{1,0:T(8,128)(2,1)} %collective-permute-done.1), channel_id=1, source_target_pairs={{0,1},{1,2},{2,3},{3,0},{4,5},{5,6},{6,7},{7,4},{8,9},{9,10},{10,1... | collective-permute-start | bytes 1572872 | tf_op jit(solution)/shard_map/ppermute | solution.py:21
  87.8 4.6 %copy-start.8 = (bf16[2048,256]{1,0:T(8,128)(2,1)S(1)}, bf16[2048,256]{1,0:T(8,128)(2,1)}, u32[]{:S(2)}) copy-start(bf16[2048,256]{1,0:T(8,128)(2,1)} %param.24) | copy-start | bytes 3145732
  90.3 2.1 copy-start.3
  92.4 1.5 copy-start.9
  93.8 71.7 %all-gather.3.cloned.1.call-start = ((), (), s32[]{:S(2)}) async-start(), calls=%async_computation.4 | async-start | bytes 1310720 | tf_op jit(solution)/shard_map/all_gather | solution.py:117
  96.9 131.1 %reduce-scatter.5.cloned.1.call-start = ((), (), s32[]{:S(2)}) async-start(), calls=%async_computation.7 | async-start | bytes 5898240 | tf_op jit(solution)/shard_map/reduce_scatter | solution.py:198
  111.8 3.7 %copy-start.7 = (bf16[1,2048,512]{2,1,0:T(8,128)(2,1)S(1)}, bf16[1,2048,512]{2,1,0:T(8,128)(2,1)}, u32[]{:S(2)}) copy-start(bf16[1,2048,512]{2,1,0:T(8,128)(2,1)} %param.31) | copy-start | bytes 6291460
  146.1 0.7 copy-start.4
  146.2 115.4 %reduce-scatter.3.cloned.1.call-start = ((), (), s32[]{:S(2)}) async-start(), calls=%async_computation.6 | async-start | bytes 2621440 | tf_op jit(solution)/shard_map/reduce_scatter | solution.py:187
  175.4 57.3 %copy-start.6 = (f32[128,2]{0,1:T(2,128)S(1)}, f32[128,2]{0,1:T(2,128)}, u32[]{:S(2)}) copy-start(f32[128,2]{0,1:T(2,128)} %param.30) | copy-start | bytes 3076
  175.4 87.5 %copy-start.5 = (f32[2048]{0:T(1024)S(1)}, f32[2048]{0:T(1024)}, u32[]{:S(2)}) copy-start(f32[2048]{0:T(1024)} %param.26) | copy-start | bytes 24580
  228.0 36.8 %all-to-all-start.1 = ((bf16[4,1,72,2048]{3,2,1,0:T(8,128)(2,1)}), bf16[4,1,72,2048]{3,2,1,0:T(8,128)(2,1)S(1)}, u32[]{:S(2)}, u32[]{:S(2)}) async-start(bf16[4,1,72,2048]{3,2,1,0:T(8,128)(2,1)} %bitcast.295), calls=%async_computation.3 | async-start | bytes 2359296 | tf_op jit(solution)/shard_map/all_to_all | solution.py:203
Sparse Core Ops, SparseCore 0:
  93.9 42.5 all-gather.4
  138.7 26.7 all-gather.2
Sparse Core Ops, SparseCore 1:
  146.3 81.7 reduce-scatter.4
  230.4 31.1 reduce-scatter.2
